TPU v7x, 256 devices: a 4x2x16 block of a 4x16x16 slice. The times are simulated.
256 devices in a mesh: grp: 2 (over y), sp: 32 (over z, core), tp: 4 (over x).
Axes of the slice: x: 4, y: 2, z: 16, core: 2. Of those that a mesh axis runs over, the one named last changes fastest.
The devices are a block of a 4x16x16 slice.
Arguments:
- queries: bfloat16 [14336, 1024], P(('grp', 'sp'), 'tp'), parts along dimension 0, may hold values from -6 to 6
- head_key_rows: bfloat16 [14336, 1024], P(('grp', 'sp'), 'tp'), parts along dimension 0, may hold values from -6 to 6
- head_value_rows: bfloat16 [14336, 2048], P(('grp', 'sp'), 'tp'), parts along dimension 0, may hold values from -6 to 6
- input_gate_logit: float32 [16, 14336], P('tp', ('grp', 'sp')), parts along dimension 1, may hold values from -6 to 300
- forget_gate_preact: float32 [16, 14336], P('tp', ('grp', 'sp')), parts along dimension 1, may hold values from 0 to 14
- forget_log_offset: float32 [16, 14336], P('tp', ('grp', 'sp')), parts along dimension 1, may hold values from -0.7 to 0
- per_head_norm_gain: bfloat16 [2048], P('tp'), may hold values from 0.099609375 to 1.8984375
- cell_output_matrix: bfloat16 [2048, 2048], P('tp', 'sp'), may hold values from -0.125 to 0.125
- layer_input_rows: bfloat16 [14336, 2048], P(('grp', 'sp', 'tp')), parts along dimension 0, may hold values from -6 to 6
- expert_norm_gain: bfloat16 [2048], replicated, may hold values from 0.099609375 to 1.8984375
- chosen_expert_index: int32 [14336, 2], P(('grp', 'sp', 'tp')), parts along dimension 0, may hold values from 0 to 31, all different within a row; in each aligned block of 56 rows (0 to 55, 56 to 111, ...) at most 7 rows name the same one
- chosen_expert_weight: float32 [14336, 2], P(('grp', 'sp', 'tp')), parts along dimension 0, may hold values from 0.2 to 1
- expert_gate_matrix: bfloat16 [32, 2048, 3584], P('sp', None, 'tp'), may hold values from -0.125 to 0.125
- expert_up_matrix: bfloat16 [32, 2048, 3584], P('sp', None, 'tp'), may hold values from -0.125 to 0.125
- expert_down_matrix: bfloat16 [32, 3584, 2048], P('sp', 'tp'), may hold values from -0.09375 to 0.09375
Outputs:
- layer_out: bfloat16 [14336, 2048], P(('grp', 'sp', 'tp')), parts along dimension 0
There are 2 independent parts, one for each index of `grp`. A program takes and returns all parts, laid end to end along the dimension named above; an argument that names none is the same for every part. Nothing has to cross between parts.
Inputs may be any that keep to these rules, and one draw needn't show every extreme that they name: `chosen_expert_index`: each row names 2 different experts. In the rows of one device no expert is named more than 7 times, and in every draw some expert is named exactly 7 times in the rows of some device.
All inputs are finite; a program needn't handle non-finite values.
Results may differ from a plain program's by a relative error of at most 0.013.
Values may be sent and summed in bfloat16 or wider, within the bound.
No kernel may reach another device: no remote copies, remote signals or barrier semaphores. Data moves between devices by JAX's collectives and lax.ppermute only.
A program may use at most 64 MiB of HBM per device.

v0:
```python
import jax
import jax.numpy as jnp
from jax import lax
from jax.sharding import Mesh
from jax.sharding import PartitionSpec as P

DK = 64
DV = 128
SP = ("sp_0", "sp_1")
GRP_SP = ("grp", "sp_0", "sp_1")
GRP_SP_TP = ("grp", "sp_0", "sp_1", "tp")
far_below = -1e30
norm_eps = 1e-06


def all_in_one(x, axis):
    leaves = jax.tree.leaves(x)
    turns = sorted(range(len(leaves)), key=lambda k: -leaves[k].size)
    width = (1, *leaves[turns[0]].shape)[-1]
    lines = [
        jnp.pad(leaves[k].reshape(-1), (0, -leaves[k].size % width)).reshape(-1, width)
        for k in turns
    ]
    both, at, found = (lax.all_gather(jnp.concatenate(lines), axis), 0, {})
    for k, line in zip(turns, lines):
        slab = both[:, at : at + len(line)].reshape(len(both), -1)
        found[k] = slab[:, : leaves[k].size].reshape(-1, *leaves[k].shape)
        at += len(line)
    numbers = iter(range(len(leaves)))
    return jax.tree.map(lambda _: found[next(numbers)], x)


def carried_in(part, axis, combine, identity):
    place = lax.axis_index(axis)
    gathered = all_in_one(part, axis)
    state = jax.tree.map(lambda a, e: jnp.zeros_like(a) + jnp.asarray(e, a.dtype), part, identity)

    def one(lap, state):
        return combine(
            state, jax.tree.map(lambda a: lax.dynamic_index_in_dim(a, lap, 0, False), gathered)
        )

    return lax.fori_loop(0, place, one, state)


def cut_along(x, dim, size):
    before, after = (x.shape[:dim], x.shape[dim + 1 :])
    return jnp.moveaxis(x.reshape(*before, size, -1, *after), dim, 0)


def summed_on_arrival(x, axis, dim):
    size = lax.axis_size(axis)
    tiles = lax.all_to_all(cut_along(x, dim, size), axis, 0, 0, tiled=True)
    return jnp.sum(tiles.astype(jnp.float32), axis=0)


def from_everyone(x, axis):
    copies = jnp.broadcast_to(x, (lax.axis_size(axis), *x.shape))
    return lax.all_to_all(copies, axis, split_axis=0, concat_axis=0, tiled=True)


def joined_along(tiles, dim):
    dims = list(tiles.shape[1:])
    dims[dim] *= tiles.shape[0]
    return jnp.moveaxis(tiles, 0, dim).reshape(dims)


def collect(x, axis, dim):
    tiles = from_everyone(x, axis)
    return joined_along(tiles, dim)


def exchange_in_order(tiles, axes, turns):
    dims = [lax.axis_size(a) for a in axes]
    tiles = tiles.reshape(*dims, *tiles.shape[1:])
    for k in turns:
        tiles = lax.all_to_all(tiles, axes[k], split_axis=k, concat_axis=k, tiled=True)
    return tiles.reshape(-1, *tiles.shape[len(axes) :])


def exchange_by_chip(x, groups, turns, split_dim, concat_dim):
    size = lax.axis_size(groups[0]) * lax.axis_size(groups[1])
    tiles = cut_along(x, split_dim, size)
    return joined_along(exchange_in_order(tiles, groups, turns), concat_dim)


def items_in_groups(x, axis, split_dim, concat_dim, work, item_dim, out_dim):
    items = jax.tree.leaves(x)[0].shape[item_dim]
    count = 2 if items % 2 == 0 else 1
    finished = []
    for k in range(count):
        group = jax.tree.map(
            lambda a: lax.slice_in_dim(
                a, k * (items // count), (k + 1) * (items // count), axis=item_dim
            ),
            x,
        )
        finished.append(
            work(
                lax.all_to_all(
                    group, axis, split_axis=split_dim, concat_axis=concat_dim, tiled=True
                )
            )
        )
    return jax.tree.map(lambda *parts: jnp.concatenate(parts, axis=out_dim), *finished)


def combine_states(earlier, later):
    total_a, memory_a, peak_a = earlier
    total_b, memory_b, peak_b = later
    peak = jnp.maximum(total_b + peak_a, peak_b)
    weight_a = jnp.exp(total_b + peak_a - peak)
    weight_b = jnp.exp(peak_b - peak)
    memory = weight_a[:, None, None] * memory_a + weight_b[:, None, None] * memory_b
    return (total_a + total_b, memory, peak)


def block_summary(keys3, values3, log_in, log_retention):
    running = jnp.cumsum(log_retention, axis=1)
    totals = running[:, -1]
    term_log = totals[:, None] - running + log_in
    peak = jnp.max(term_log, axis=1)
    factors = jnp.transpose(jnp.exp(term_log - peak[:, None]))
    keys32 = keys3.astype(jnp.float32)
    weighted = values3.astype(jnp.float32) * factors[:, :, None]
    memory = jnp.einsum("shd,she->hde", keys32, weighted, precision=lax.Precision.HIGHEST)
    return (totals, memory, peak)


def block_output(queries3, keys3, values3, log_in, log_retention, state, gains):
    count = queries3.shape[0]
    heads = queries3.shape[1]
    memory_in, peak_in = (state[1], state[2])
    running = jnp.cumsum(log_retention, axis=1)
    rows_at = lax.broadcasted_iota(jnp.int32, (count, count), 0)
    cols_at = lax.broadcasted_iota(jnp.int32, (count, count), 1)
    causal = (cols_at <= rows_at)[None]
    decay_log = jnp.where(
        causal, running[:, :, None] - running[:, None, :] + log_in[:, None, :], far_below
    )
    carried_log = running + peak_in[:, None]
    peak = jnp.maximum(carried_log, jnp.max(decay_log, axis=2))
    qk_scale = queries3.shape[2] ** (-0.5)
    scores = (
        jnp.einsum("thd,shd->hts", queries3, keys3, preferred_element_type=jnp.float32) * qk_scale
    )
    strength = scores * jnp.exp(decay_log - peak[:, :, None])
    carried = jnp.exp(carried_log - peak)
    queries32 = queries3.astype(jnp.float32)
    from_memory = (
        jnp.einsum("thd,hde->the", queries32, memory_in, precision=lax.Precision.HIGHEST) * qk_scale
    )
    within = jnp.einsum(
        "hts,she->the", strength.astype(jnp.bfloat16), values3, preferred_element_type=jnp.float32
    )
    result = within + jnp.transpose(carried)[:, :, None] * from_memory
    result = result * lax.rsqrt(jnp.mean(result * result, axis=2, keepdims=True) + norm_eps)
    result = result * gains.astype(jnp.float32).reshape(heads, -1)
    return result.reshape(count, -1).astype(jnp.bfloat16)


def run_expert(rows_in, expert_gate_matrix, expert_up_matrix, expert_down_matrix):
    gate = jnp.dot(rows_in, expert_gate_matrix[0], preferred_element_type=jnp.float32)
    upward = jnp.dot(rows_in, expert_up_matrix[0], preferred_element_type=jnp.float32)
    hidden = (jax.nn.silu(gate) * upward).astype(jnp.bfloat16)
    return jnp.dot(hidden, expert_down_matrix[0], preferred_element_type=jnp.float32)


def shards(
    queries,
    head_key_rows,
    head_value_rows,
    input_gate_logit,
    forget_gate_preact,
    forget_log_offset,
    per_head_norm_gain,
    cell_output_matrix,
    layer_input_rows,
    expert_norm_gain,
    chosen_expert_index,
    chosen_expert_weight,
    expert_gate_matrix,
    expert_up_matrix,
    expert_down_matrix,
):
    count = queries.shape[0]
    heads = input_gate_logit.shape[0]
    queries3 = queries.reshape(count, heads, DK)
    keys3 = head_key_rows.reshape(count, heads, DK)
    values3 = head_value_rows.reshape(count, heads, DV)
    log_retention = jax.nn.log_sigmoid(forget_gate_preact) + forget_log_offset
    summary = block_summary(keys3, values3, input_gate_logit, log_retention)
    identity = (
        jnp.zeros((heads,), jnp.float32),
        jnp.zeros((heads, DK, DV), jnp.float32),
        jnp.full((heads,), far_below, jnp.float32),
    )
    incoming = carried_in(summary, SP, combine_states, identity)
    mixed = block_output(
        queries3, keys3, values3, input_gate_logit, log_retention, incoming, per_head_norm_gain
    )
    partial_value = jnp.dot(
        mixed,
        lax.all_gather(cell_output_matrix, SP, axis=1, tiled=True),
        preferred_element_type=jnp.float32,
    )
    projected = summed_on_arrival(partial_value.astype(jnp.bfloat16), "tp", 0)
    residual = layer_input_rows.astype(jnp.float32) + projected
    normed = residual * lax.rsqrt(jnp.mean(residual * residual, axis=1, keepdims=True) + norm_eps)
    normed = (normed * expert_norm_gain.astype(jnp.float32)).astype(jnp.bfloat16)
    rows = layer_input_rows.shape[0]
    model_width = layer_input_rows.shape[1]
    experts = lax.axis_size(SP)
    slots = max(2, (4 * rows + experts - 1) // experts)
    flat_ids = chosen_expert_index.reshape(rows * 2)
    onehot = (flat_ids[:, None] == jnp.arange(experts, dtype=jnp.int32)[None, :]).astype(jnp.int32)
    position = jnp.sum(jnp.cumsum(onehot, axis=0) * onehot, axis=1) - 1
    slot_index = (flat_ids * slots + position).reshape(rows, 2)
    targets = jnp.arange(experts * slots, dtype=jnp.int32)
    placing = jnp.any(slot_index[None, :, :] == targets[:, None, None], axis=2).astype(jnp.bfloat16)
    outgoing = jnp.dot(placing, normed, preferred_element_type=jnp.float32).astype(jnp.bfloat16)
    outgoing = outgoing.reshape(experts, slots, model_width)

    def expert_rows(block):
        spread = collect(block, "tp", 0)
        produced = run_expert(
            spread.reshape(-1, model_width),
            expert_gate_matrix,
            expert_up_matrix,
            expert_down_matrix,
        )
        summed = summed_on_arrival(produced.reshape(spread.shape).astype(jnp.bfloat16), "tp", 0)
        return exchange_by_chip(summed.astype(jnp.bfloat16), ("sp_0", "sp_1"), (1, 0), 0, 0)

    expert_out = items_in_groups(outgoing, SP, 0, 0, expert_rows, 1, 1)
    flat_out = expert_out.reshape(experts * slots, model_width)
    picked = jnp.take(flat_out, slot_index, axis=0).astype(jnp.float32)
    routed = jnp.sum(chosen_expert_weight[:, :, None] * picked, axis=1)
    return (residual + routed).astype(jnp.bfloat16)


def solution(mesh):
    torus = Mesh(
        mesh.devices.reshape(mesh.shape["grp"], 16, 2, mesh.shape["tp"]),
        ("grp", "sp_0", "sp_1", "tp"),
    )
    return jax.shard_map(
        shards,
        mesh=torus,
        in_specs=(
            P(GRP_SP, "tp"),
            P(GRP_SP, "tp"),
            P(GRP_SP, "tp"),
            P("tp", GRP_SP),
            P("tp", GRP_SP),
            P("tp", GRP_SP),
            P("tp"),
            P("tp", SP),
            P(GRP_SP_TP, None),
            P(),
            P(GRP_SP_TP, None),
            P(GRP_SP_TP, None),
            P(SP, None, "tp"),
            P(SP, None, "tp"),
            P(SP, "tp", None),
        ),
        out_specs=P(GRP_SP_TP, None),
        check_vma=False,
    )
```

profile of v0, /device:TPU:40, one launch (start us, length us, event | category | flops | bytes accessed | tf_op | source)
XLA Modules:
  0.0 451.1 jit_solution(10542415822173141416)
XLA Ops:
  6.6 0.8 fusion.49
  7.3 1.2 reduce-window.6
  9.2 0.9 fusion.55
  10.0 0.8 exponential_bitcast_fusion
  10.8 1.0 copy.81
  14.6 1.0 copy.80
  15.6 0.8 copy.88
  16.5 1.1 fusion.25
  17.6 80.7 %all-gather.7.cloned.1.call-done = f32[32,258,128]{2,1,0:T(8,128)} async-done(((f32[1,258,128]{2,1,0:T(8,128)}), f32[32,258,128]{2,1,0:T(8,128)}) %all-gather.7.cloned.1.call-update) | async-done | bytes 4227088 | tf_op jit(solution)/shard_map/all_gather | solution.py:24
  98.2 4.6 %slice.46 = f32[32,256,128]{2,1,0:T(8,128)} slice(f32[32,258,128]{2,1,0:T(8,128)} %all-gather.7.cloned.1.call-done), slice={[0:32], [0:256], [0:128]} | slice | bytes 8388608 | tf_op jit(solution)/shard_map/slice | solution.py:26
  102.9 1.0 fusion.54
  104.4 0.7 multiply_reduce_fusion.2
  105.2 62.1 %all-gather.5.cloned.1.call-done = bf16[512,2048]{0,1:T(8,128)(2,1)} async-done(((bf16[512,64]{0,1:T(8,128)(2,1)}), bf16[512,2048]{0,1:T(8,128)(2,1)}) %all-gather.5.cloned.1.call-update) | async-done | bytes 2097168 | tf_op jit(solution)/shard_map/all_gather | solution.py:204
  167.4 3.3 convolution_convert_fusion
  170.7 4.3 all-to-all-start
  175.7 13.3 %all-to-all-done = bf16[4,56,2048]{2,1,0:T(8,128)(2,1)S(1)} async-done(((bf16[4,56,2048]{2,1,0:T(8,128)(2,1)}), bf16[4,56,2048]{2,1,0:T(8,128)(2,1)S(1)}, u32[]{:S(2)}, u32[]{:S(2)}) %all-to-all-start) | async-done | bytes 917536 | tf_op jit(solution)/shard_map/all_to_all | solution.py:53
  190.2 64.3 %all_to_all.30 = bf16[32,7,2048]{2,1,0:T(8,128)(2,1)S(1)} all-to-all(bf16[32,7,2048]{2,1,0:T(8,128)(2,1)S(1)} %reshape.114), channel_id=1, replica_groups=mesh['grp'=2,'sp_0'=16,'sp_1'=2,'tp'=4] {'sp_0','sp_1'}, dimensions={0} | all-to-all | bytes 1835008 | tf_op jit(solution)/shard_map/all_to_all | solution.py:100
  255.5 46.2 %all_to_all.31 = bf16[4,32,7,2048]{3,1,2,0:T(8,128)(2,1)S(1)} all-to-all(bf16[4,32,7,2048]{3,1,2,0:T(8,128)(2,1)S(1)} %broadcast_in_dim.53), channel_id=1, replica_groups=mesh['grp'=2,'sp_0'=16,'sp_1'=2,'tp'=4] {'tp'}, dimensions={0} | all-to-all | bytes 7340032 | tf_op jit(solution)/shard_map/all_to_all | solution.py:59
  301.7 4.0 copy.92
  305.7 6.0 %reshape_reshape.10 = bf16[896,2048]{1,0:T(8,128)(2,1)} reshape(bf16[4,32,7,2048]{3,2,1,0:T(8,128)(2,1)} %copy.92) | data formatting | bytes 7340032 | tf_op jit(solution)/shard_map/reshape;reshape | solution.py:227
  311.8 7.2 %fusion.7 = f32[896,896]{1,0:T(8,128)S(1)} fusion(bf16[896,2048]{1,0:T(8,128)(2,1)} %reshape_reshape.10, bf16[1,2048,896]{2,1,0:T(8,128)(2,1)} %param.30), kind=kOutput, calls=%fused_computation.13 | convolution fusion | flops 3288334336 | bytes 10551296 | tf_op jit(solution)/shard_map/dot_general | solution.py:164
  319.0 5.4 %multiply_convert_fusion = bf16[896,896]{1,0:T(8,128)(2,1)} fusion(f32[896,896]{1,0:T(8,128)S(1)} %fusion.7, bf16[896,2048]{1,0:T(8,128)(2,1)S(1)} %copy-done.2, bf16[1,2048,896]{2,1,0:T(8,128)(2,1)S(1)} %copy-done.8), kind=kOutput, calls=%fused_computation.18 | convolution fusion | flops 3293151232 | bytes 12156928 | tf_op jit(solution)/shard_map/dot_general | solution.py:163
  324.4 2.5 dot_general.40
  326.9 6.2 %fusion.11 = bf16[128,7,2048]{2,0,1:T(8,128)(2,1)S(1)} fusion(bf16[1,896,2048]{2,1,0:T(8,128)(2,1)} %param.31, bf16[128,7,896]{2,1,0:T(8,128)(2,1)S(1)} %dot_general.40), kind=kOutput, calls=%fused_computation.17 | convolution fusion | flops 3290169344 | bytes 8945664 | tf_op jit(solution)/shard_map/dot_general | solution.py:166
  333.6 46.2 %all_to_all.32 = bf16[4,32,7,2048]{3,1,2,0:T(8,128)(2,1)} all-to-all(bf16[4,32,7,2048]{3,1,2,0:T(8,128)(2,1)S(1)} %copy.94), channel_id=1, replica_groups=mesh['grp'=2,'sp_0'=16,'sp_1'=2,'tp'=4] {'tp'}, dimensions={0} | all-to-all | bytes 7340032 | tf_op jit(solution)/shard_map/all_to_all | solution.py:53
  379.8 2.8 reduce_sum.61
  383.5 4.5 all_to_all.33
  388.0 1.9 copy.97
  389.8 4.3 all-to-all-start.5
  394.6 44.8 %all-to-all-done.5 = bf16[16,2,1,7,2048]{4,1,3,2,0:T(2,128)(2,1)S(1)} async-done(((bf16[16,2,1,7,2048]{4,1,3,2,0:T(2,128)(2,1)}), bf16[16,2,1,7,2048]{4,1,3,2,0:T(2,128)(2,1)S(1)}, u32[]{:S(2)}, u32[]{:S(2)}) %all-to-all-start.5) | async-done | bytes 917536 | tf_op jit(solution)/shard_map/all_to_all | solution.py:77
  440.1 0.9 gather_fusion
  441.3 2.2 multiply_reduce_fusion
  (73 shorter events, 10.3 us)
Async XLA Ops:
  6.5 5.3 %copy-start = (bf16[224,512]{1,0:T(8,128)(2,1)S(1)}, bf16[224,512]{1,0:T(8,128)(2,1)}, u32[]{:S(2)}) copy-start(bf16[224,512]{1,0:T(8,128)(2,1)} %param.19) | copy-start | bytes 688132
  6.6 91.7 %all-gather.7.cloned.1.call-start = ((), (), s32[]{:S(2)}) async-start(), calls=%async_computation.7 | async-start | bytes 4460544 | tf_op jit(solution)/shard_map/all_gather | solution.py:24
  13.0 154.3 %all-gather.5.cloned.1.call-start = ((), (), s32[]{:S(2)}) async-start(), calls=%async_computation.6 | async-start | bytes 2162688 | tf_op jit(solution)/shard_map/all_gather | solution.py:204
  17.6 86.8 %copy-start.4 = (f32[4,224]{1,0:T(4,128)S(1)}, f32[4,224]{1,0:T(4,128)}, u32[]{:S(2)}) copy-start(f32[4,224]{1,0:T(4,128)} %param.20) | copy-start | bytes 10756
  104.4 71.2 %copy-start.5 = (bf16[2048]{0:T(1024)(128)(2,1)S(1)}, bf16[2048]{0:T(1024)(128)(2,1)}, u32[]{:S(2)}) copy-start(bf16[2048]{0:T(1024)(128)(2,1)} %param.26) | copy-start | bytes 12292
  104.4 71.2 %copy-start.6 = (s32[56,2]{0,1:T(2,128)S(1)}, s32[56,2]{0,1:T(2,128)}, u32[]{:S(2)}) copy-start(s32[56,2]{0,1:T(2,128)} %param.27) | copy-start | bytes 1348
  105.2 84.0 %copy-start.3 = (bf16[56,2048]{1,0:T(8,128)(2,1)S(1)}, bf16[56,2048]{1,0:T(8,128)(2,1)}, u32[]{:S(2)}) copy-start(bf16[56,2048]{1,0:T(8,128)(2,1)} %param.25) | copy-start | bytes 688132
  170.7 18.3 %all-to-all-start = ((bf16[4,56,2048]{2,1,0:T(8,128)(2,1)}), bf16[4,56,2048]{2,1,0:T(8,128)(2,1)S(1)}, u32[]{:S(2)}, u32[]{:S(2)}) async-start(bf16[4,56,2048]{2,1,0:T(8,128)(2,1)} %bitcast.19), calls=%async_computation | async-start | bytes 1835008 | tf_op jit(solution)/shard_map/all_to_all | solution.py:53
  311.8 7.2 %copy-start.2 = (bf16[896,2048]{1,0:T(8,128)(2,1)S(1)}, bf16[896,2048]{1,0:T(8,128)(2,1)}, u32[]{:S(2)}) copy-start(bf16[896,2048]{1,0:T(8,128)(2,1)} %reshape_reshape.10) | copy-start | bytes 11010052
  311.8 7.3 %copy-start.8 = (bf16[1,2048,896]{2,1,0:T(8,128)(2,1)S(1)}, bf16[1,2048,896]{2,1,0:T(8,128)(2,1)}, u32[]{:S(2)}) copy-start(bf16[1,2048,896]{2,1,0:T(8,128)(2,1)} %param.29) | copy-start | bytes 11010052
  383.2 11.3 %copy-start.7 = (f32[56,2]{0,1:T(2,128)S(1)}, f32[56,2]{0,1:T(2,128)}, u32[]{:S(2)}) copy-start(f32[56,2]{0,1:T(2,128)} %param.28) | copy-start | bytes 1348
  389.8 49.6 %all-to-all-start.5 = ((bf16[16,2,1,7,2048]{4,1,3,2,0:T(2,128)(2,1)}), bf16[16,2,1,7,2048]{4,1,3,2,0:T(2,128)(2,1)S(1)}, u32[]{:S(2)}, u32[]{:S(2)}) async-start(bf16[16,2,1,7,2048]{4,1,3,2,0:T(2,128)(2,1)} %copy.97), calls=%async_computation.5 | async-start | bytes 1835008 | tf_op jit(solution)/shard_map/all_to_all | solution.py:77
  439.8 4.5 copy-start.1
Sparse Core Ops, SparseCore 0:
  13.2 85.0 all-gather.6
  100.1 67.2 all-gather.4
where the time goes:
time: 453 us; the launch traced here: 451 us
  waiting for transfers between devices  202 us (45%)
  blocking collectives  161 us (36%)
  local copies, waits for them, and re-layouts  28.6 us (6%)
  matrix products  24.3 us (5%)
  between operations  13.8 us (3%)
  other arithmetic  12.9 us (3%)
  starting transfers between devices  8.63 us (2%)
    all_gather x1, waiting for transfers between devices, all_in_one(): both, at, found = (lax.all_gather(jnp.concatenate(lines), axis), 0, {})  80.7 us
    all_to_all x1, blocking collectives, items_in_groups(): lax.all_to_all(group, axis, split_axis=split_dim, concat_axis=concat_dim,...  64.3 us
    all_gather x1, waiting for transfers between devices, shards(): lax.all_gather(cell_output_matrix, SP, axis=1, tiled=True)  62.1 us
    all_to_all x1, blocking collectives, from_everyone(): return lax.all_to_all(copies, axis, split_axis=0, concat_axis=0, tiled=True)  46.2 us
    all_to_all x1, blocking collectives, summed_on_arrival(): tiles = lax.all_to_all(cut_along(x, dim, size), axis, 0, 0, tiled=True)  46.2 us
    all_to_all x1, waiting for transfers between devices, exchange_in_order(): lax.all_to_all(tiles, axes[k], split_axis=k, concat_axis=k, tiled=True)  44.8 us
    all_to_all x1, waiting for transfers between devices, summed_on_arrival(): tiles = lax.all_to_all(cut_along(x, dim, size), axis, 0, 0, tiled=True)  13.3 us
  transfers between devices with their start and end apart: 4, of which 4 were waited for; matrix products, arithmetic and copies ran while one was open for 3% of the time, Pallas kernels for 0%

commit v1 on v0

--- a/solution.py
+++ b/solution.py
@@ -201,7 +201,9 @@
     )
     partial_value = jnp.dot(
         mixed,
-        lax.all_gather(cell_output_matrix, SP, axis=1, tiled=True),
+        jnp.concatenate(
+            lax.all_to_all(jnp.stack([cell_output_matrix] * lax.axis_size(SP)), SP, 0, 0), axis=1
+        ),
         preferred_element_type=jnp.float32,
     )
     projected = summed_on_arrival(partial_value.astype(jnp.bfloat16), "tp", 0)

time: 453 us -> 475 us (1.049)
  blocking collectives: 161 us -> 189 us
  waiting for transfers between devices: 202 us -> 175 us
  starting transfers between devices: 8.63 us -> 33.3 us
    all_gather x1 -> x0, waiting for transfers between devices: 62.1 us -> none  [shards(): lax.all_gather(cell_output_matrix, SP, axis=1, tiled=True)]
    all_gather x1, waiting for transfers between devices: 80.7 us -> 115 us  [all_in_one(): both, at, found = (lax.all_gather(jnp.concatenate(lines), axis), 0, {})]
    all_to_all x1, blocking collectives: 64.3 us -> 91.9 us  [items_in_groups(): lax.all_to_all(group, axis, split_axis=split_dim, concat_axis=concat_dim,...]
    all_to_all x0 -> x1, starting transfers between devices: none -> 24.7 us  [shards(): lax.all_to_all(jnp.stack([cell_output_matrix] * lax.axis_size(SP)), SP, 0...]
  transfers between devices with their start and end apart: 4 -> 4, of which waited for: 4 -> 3; matrix products, arithmetic and copies ran while one was open for 3% -> 3% of each run, Pallas kernels for 0% -> 0%
where the time goes in v1:
time: 475 us; the launch traced here: 474 us
  blocking collectives  189 us (40%)
  waiting for transfers between devices  175 us (37%)
  starting transfers between devices  33.3 us (7%)
  local copies, waits for them, and re-layouts  29.1 us (6%)
  matrix products  22.7 us (5%)
  between operations  13.9 us (3%)
  other arithmetic  11.5 us (2%)
    all_gather x1, waiting for transfers between devices, all_in_one(): both, at, found = (lax.all_gather(jnp.concatenate(lines), axis), 0, {})  115 us
    all_to_all x1, blocking collectives, items_in_groups(): lax.all_to_all(group, axis, split_axis=split_dim, concat_axis=concat_dim,...  91.9 us
    all_to_all x1, blocking collectives, from_everyone(): return lax.all_to_all(copies, axis, split_axis=0, concat_axis=0, tiled=True)  46.2 us
    all_to_all x1, blocking collectives, summed_on_arrival(): tiles = lax.all_to_all(cut_along(x, dim, size), axis, 0, 0, tiled=True)  46.2 us
    all_to_all x1, waiting for transfers between devices, exchange_in_order(): lax.all_to_all(tiles, axes[k], split_axis=k, concat_axis=k, tiled=True)  45.3 us
    all_to_all x1, starting transfers between devices, shards(): lax.all_to_all(jnp.stack([cell_output_matrix] * lax.axis_size(SP)), SP, 0...  24.7 us
    all_to_all x1, waiting for transfers between devices, summed_on_arrival(): tiles = lax.all_to_all(cut_along(x, dim, size), axis, 0, 0, tiled=True)  14.3 us
  transfers between devices with their start and end apart: 4, of which 3 were waited for; matrix products, arithmetic and copies ran while one was open for 3% of the time, Pallas kernels for 0%

profile of v1, /device:TPU:40, one launch (start us, length us, event | category | flops | bytes accessed | tf_op | source)
XLA Modules:
  0.0 474.0 jit_solution(7300180685984158342)
XLA Ops:
  6.6 0.8 fusion.49
  7.3 1.2 reduce-window.6
  9.2 0.9 fusion.55
  10.0 0.8 exponential_bitcast_fusion
  10.8 1.0 copy.82
  12.4 0.7 maximum_bitcast_fusion
  13.1 2.4 stack.2
  15.5 24.7 %all-to-all-start = ((bf16[32,512,64]{1,2,0:T(8,128)(2,1)}), bf16[32,512,64]{1,2,0:T(8,128)(2,1)S(1)}, u32[]{:S(2)}, u32[]{:S(2)}) async-start(bf16[32,512,64]{1,2,0:T(8,128)(2,1)} %stack.2), calls=%async_computation | async-start | bytes 4194304 | tf_op jit(solution)/shard_map/all_to_all | solution.py:205
  41.7 115.1 %all-gather.4.cloned.1.call-done = f32[32,258,128]{2,1,0:T(8,128)} async-done(((f32[1,258,128]{2,1,0:T(8,128)}), f32[32,258,128]{2,1,0:T(8,128)}) %all-gather.4.cloned.1.call-update) | async-done | bytes 4227088 | tf_op jit(solution)/shard_map/all_gather | solution.py:24
  156.8 4.6 slice.46
  161.4 1.0 fusion.54
  163.0 1.7 multiply_reduce_fusion.2
  164.6 1.8 convolution_convert_fusion
  166.4 4.4 all-to-all-start.1
  171.6 14.3 %all-to-all-done.1 = bf16[4,56,2048]{2,1,0:T(8,128)(2,1)S(1)} async-done(((bf16[4,56,2048]{2,1,0:T(8,128)(2,1)}), bf16[4,56,2048]{2,1,0:T(8,128)(2,1)S(1)}, u32[]{:S(2)}, u32[]{:S(2)}) %all-to-all-start.1) | async-done | bytes 917536 | tf_op jit(solution)/shard_map/all_to_all | solution.py:53
  187.0 91.9 %all_to_all.35 = bf16[32,7,2048]{2,1,0:T(8,128)(2,1)S(1)} all-to-all(bf16[32,7,2048]{2,1,0:T(8,128)(2,1)S(1)} %reshape.124), channel_id=1, replica_groups=mesh['grp'=2,'sp_0'=16,'sp_1'=2,'tp'=4] {'sp_0','sp_1'}, dimensions={0} | all-to-all | bytes 1835008 | tf_op jit(solution)/shard_map/all_to_all | solution.py:100
  279.9 46.2 %all_to_all.36 = bf16[4,32,7,2048]{3,1,2,0:T(8,128)(2,1)S(1)} all-to-all(bf16[4,32,7,2048]{3,1,2,0:T(8,128)(2,1)S(1)} %broadcast_in_dim.53), channel_id=1, replica_groups=mesh['grp'=2,'sp_0'=16,'sp_1'=2,'tp'=4] {'tp'}, dimensions={0} | all-to-all | bytes 7340032 | tf_op jit(solution)/shard_map/all_to_all | solution.py:59
  326.1 4.0 copy.93
  330.1 6.0 %reshape_reshape.10 = bf16[896,2048]{1,0:T(8,128)(2,1)} reshape(bf16[4,32,7,2048]{3,2,1,0:T(8,128)(2,1)} %copy.93) | data formatting | bytes 7340032 | tf_op jit(solution)/shard_map/reshape;reshape | solution.py:229
  336.1 7.2 %fusion.7 = f32[896,896]{1,0:T(8,128)S(1)} fusion(bf16[896,2048]{1,0:T(8,128)(2,1)} %reshape_reshape.10, bf16[1,2048,896]{2,1,0:T(8,128)(2,1)} %param.30), kind=kOutput, calls=%fused_computation.13 | convolution fusion | flops 3288334336 | bytes 10551296 | tf_op jit(solution)/shard_map/dot_general | solution.py:164
  343.4 4.2 multiply_convert_fusion
  347.6 1.5 dot_general.40
  349.1 6.5 %fusion.11 = bf16[128,7,2048]{2,0,1:T(8,128)(2,1)S(1)} fusion(bf16[1,896,2048]{2,1,0:T(8,128)(2,1)} %param.31, bf16[128,7,896]{2,1,0:T(8,128)(2,1)} %dot_general.40), kind=kOutput, calls=%fused_computation.17 | convolution fusion | flops 3290169344 | bytes 8945664 | tf_op jit(solution)/shard_map/dot_general | solution.py:166
  356.2 46.2 %all_to_all.37 = bf16[4,32,7,2048]{3,1,2,0:T(8,128)(2,1)} all-to-all(bf16[4,32,7,2048]{3,1,2,0:T(8,128)(2,1)S(1)} %copy.95), channel_id=1, replica_groups=mesh['grp'=2,'sp_0'=16,'sp_1'=2,'tp'=4] {'tp'}, dimensions={0} | all-to-all | bytes 7340032 | tf_op jit(solution)/shard_map/all_to_all | solution.py:53
  402.3 2.8 reduce_sum.61
  406.0 4.5 all_to_all.38
  410.5 1.9 copy.98
  412.4 4.1 all-to-all-start.6
  416.9 45.3 %all-to-all-done.6 = bf16[16,2,1,7,2048]{4,1,3,2,0:T(2,128)(2,1)S(1)} async-done(((bf16[16,2,1,7,2048]{4,1,3,2,0:T(2,128)(2,1)}), bf16[16,2,1,7,2048]{4,1,3,2,0:T(2,128)(2,1)S(1)}, u32[]{:S(2)}, u32[]{:S(2)}) %all-to-all-start.6) | async-done | bytes 917536 | tf_op jit(solution)/shard_map/all_to_all | solution.py:77
  463.0 0.9 gather_fusion
  464.2 2.2 multiply_reduce_fusion
  466.4 0.7 add_convert_fusion
  (83 shorter events, 8.7 us)
Async XLA Ops:
  6.5 5.3 %copy-start = (bf16[224,512]{1,0:T(8,128)(2,1)S(1)}, bf16[224,512]{1,0:T(8,128)(2,1)}, u32[]{:S(2)}) copy-start(bf16[224,512]{1,0:T(8,128)(2,1)} %param.19) | copy-start | bytes 688132
  6.6 150.2 %all-gather.4.cloned.1.call-start = ((), (), s32[]{:S(2)}) async-start(), calls=%async_computation.7 | async-start | bytes 4460544 | tf_op jit(solution)/shard_map/all_gather | solution.py:24
  11.8 3.7 copy-start.6
  11.8 28.5 %copy-start.7 = (bf16[224,256]{1,0:T(8,128)(2,1)S(1)}, bf16[224,256]{1,0:T(8,128)(2,1)}, u32[]{:S(2)}) copy-start(bf16[224,256]{1,0:T(8,128)(2,1)} %param.17) | copy-start | bytes 344068
  11.8 28.6 %copy-start.10 = (s32[56,2]{0,1:T(2,128)S(1)}, s32[56,2]{0,1:T(2,128)}, u32[]{:S(2)}) copy-start(s32[56,2]{0,1:T(2,128)} %param.27) | copy-start | bytes 1348
  12.3 29.0 %copy-start.8 = (f32[4,224]{1,0:T(4,128)S(1)}, f32[4,224]{1,0:T(4,128)}, u32[]{:S(2)}) copy-start(f32[4,224]{1,0:T(4,128)} %param.20) | copy-start | bytes 10756
  12.4 29.3 %copy-start.11 = (bf16[512]{0:T(512)(128)(2,1)S(1)}, bf16[512]{0:T(512)(128)(2,1)}, u32[]{:S(2)}) copy-start(bf16[512]{0:T(512)(128)(2,1)} %param.23) | copy-start | bytes 3076
  15.5 149.1 %all-to-all-start = ((bf16[32,512,64]{1,2,0:T(8,128)(2,1)}), bf16[32,512,64]{1,2,0:T(8,128)(2,1)S(1)}, u32[]{:S(2)}, u32[]{:S(2)}) async-start(bf16[32,512,64]{1,2,0:T(8,128)(2,1)} %stack.2), calls=%async_computation | async-start | bytes 4194304 | tf_op jit(solution)/shard_map/all_to_all | solution.py:205
  40.7 0.6 copy-start.5
  162.9 8.5 %copy-start.9 = (bf16[2048]{0:T(1024)(128)(2,1)S(1)}, bf16[2048]{0:T(1024)(128)(2,1)}, u32[]{:S(2)}) copy-start(bf16[2048]{0:T(1024)(128)(2,1)} %param.26) | copy-start | bytes 12292
  164.6 21.4 %copy-start.3 = (bf16[56,2048]{1,0:T(8,128)(2,1)S(1)}, bf16[56,2048]{1,0:T(8,128)(2,1)}, u32[]{:S(2)}) copy-start(bf16[56,2048]{1,0:T(8,128)(2,1)} %param.25) | copy-start | bytes 688132
  166.4 19.5 %all-to-all-start.1 = ((bf16[4,56,2048]{2,1,0:T(8,128)(2,1)}), bf16[4,56,2048]{2,1,0:T(8,128)(2,1)S(1)}, u32[]{:S(2)}, u32[]{:S(2)}) async-start(bf16[4,56,2048]{2,1,0:T(8,128)(2,1)} %bitcast.21), calls=%async_computation.1 | async-start | bytes 1835008 | tf_op jit(solution)/shard_map/all_to_all | solution.py:53
  336.1 7.2 %copy-start.2 = (bf16[896,2048]{1,0:T(8,128)(2,1)S(1)}, bf16[896,2048]{1,0:T(8,128)(2,1)}, u32[]{:S(2)}) copy-start(bf16[896,2048]{1,0:T(8,128)(2,1)} %reshape_reshape.10) | copy-start | bytes 11010052
  336.1 7.2 %copy-start.13 = (bf16[1,2048,896]{2,1,0:T(8,128)(2,1)S(1)}, bf16[1,2048,896]{2,1,0:T(8,128)(2,1)}, u32[]{:S(2)}) copy-start(bf16[1,2048,896]{2,1,0:T(8,128)(2,1)} %param.29) | copy-start | bytes 11010052
  405.7 11.1 %copy-start.12 = (f32[56,2]{0,1:T(2,128)S(1)}, f32[56,2]{0,1:T(2,128)}, u32[]{:S(2)}) copy-start(f32[56,2]{0,1:T(2,128)} %param.28) | copy-start | bytes 1348
  412.4 49.9 %all-to-all-start.6 = ((bf16[16,2,1,7,2048]{4,1,3,2,0:T(2,128)(2,1)}), bf16[16,2,1,7,2048]{4,1,3,2,0:T(2,128)(2,1)S(1)}, u32[]{:S(2)}, u32[]{:S(2)}) async-start(bf16[16,2,1,7,2048]{4,1,3,2,0:T(2,128)(2,1)} %copy.98), calls=%async_computation.6 | async-start | bytes 1835008 | tf_op jit(solution)/shard_map/all_to_all | solution.py:77
  462.6 3.8 copy-start.4
  462.6 4.5 copy-start.1
Sparse Core Ops, SparseCore 0:
  13.2 143.5 all-gather.3
